TPU v7x, 128 devices: a whole 4x4x4 slice. The times are simulated.
128 devices in a mesh: ep: 32 (over z, y, core), tp: 4 (over x).
Axes of the slice: x: 4, y: 4, z: 4, core: 2. Of those that a mesh axis runs over, the one named last changes fastest.
Arguments:
- query_rows: bfloat16 [32768, 1024], P('ep', 'tp'), may hold values from -140 to 140
- key_rows: bfloat16 [32768, 256], P('ep', 'tp'), may hold values from -4.5 to 4.5
- value_rows: bfloat16 [32768, 256], P('ep', 'tp'), may hold values from -6 to 6
- sink_logit: float32 [16], P('tp'), may hold values from 1 to 6
- out_weight: bfloat16 [1024, 2048], P('tp'), may hold values from -0.1875 to 0.1875
- routed_rows: bfloat16 [16384, 2048], P(('ep', 'tp')), may hold values from -6 to 6
- norm_gain: float32 [2048], replicated, may hold values from 0.1 to 1.9
- routing: int32 [16384, 2], P(('ep', 'tp')), may hold values from 0 to 31, all different within a row; in each aligned block of 128 rows (0 to 127, 128 to 255, ...) at most 9 rows name the same one
- route_weight: float32 [16384, 2], P(('ep', 'tp')), may hold values from 0.2 to 1
- gate_weight: bfloat16 [32, 2048, 7168], P('ep', None, 'tp'), may hold values from -0.125 to 0.125
- up_weight: bfloat16 [32, 2048, 7168], P('ep', None, 'tp'), may hold values from -0.125 to 0.125
- down_weight: bfloat16 [32, 7168, 2048], P('ep', 'tp'), may hold values from -0.0625 to 0.0625
Outputs:
- mixed_rows: bfloat16 [32768, 2048], P(('ep', 'tp'))
- expert_mix: bfloat16 [16384, 2048], P(('ep', 'tp'))
Inputs may be any that keep to these rules, and one draw needn't show every extreme that they name: `routing`: each token names 2 different experts. Within the 128 rows of one device no expert is named by more than 9 rows, and in every draw some device's rows name some expert exactly 9 times.
All inputs are finite; a program needn't handle non-finite values.
Results may differ from a plain program's by a relative error of at most 0.012.
Values may be sent and summed in bfloat16 or wider, within the bound.
A program may use at most 128 MiB of HBM per device.

v0:
```python
import jax
import jax.numpy as jnp
from jax import lax
from jax.sharding import PartitionSpec as P

HEAD_DIM = 64
WINDOW = 128


EPS = 1e-06


def padded_2(value, sides, width):
    for axis, dim in sides:
        peers, length = (lax.axis_size(axis), value.shape[dim])
        up = [(i, (i + 1) % peers) for i in range(peers - 1)]
        down = [(j, i) for i, j in up]
        last = lax.slice_in_dim(value, length - width, length, axis=dim)
        leading = lax.slice_in_dim(value, 0, width, axis=dim)
        before = lax.ppermute(last, axis, up)
        after = lax.ppermute(leading, axis, down)
        value = jnp.concatenate([before, value, after], axis=dim)
    return value


def split_up(value, dim, peers):
    dims = value.shape
    pieces = value.reshape(*dims[:dim], peers, dims[dim] // peers, *dims[dim + 1 :])
    return jnp.moveaxis(pieces, dim, 0)


def sum_at_owner(value, axis, dim):
    peers = lax.axis_size(axis)
    pieces = lax.all_to_all(split_up(value, dim, peers), axis, 0, 0, tiled=True)
    return jnp.sum(pieces.astype(jnp.float32), axis=0)


def items_in_groups(value, axis, split_dim, concat_dim, work, item_dim, out_dim):
    items = jax.tree.leaves(value)[0].shape[item_dim]
    count = 4 if items % 4 == 0 else 1
    done = []
    for k in range(count):
        group = jax.tree.map(
            lambda a: lax.slice_in_dim(
                a, k * (items // count), (k + 1) * (items // count), axis=item_dim
            ),
            value,
        )
        done.append(
            work(
                lax.all_to_all(
                    group, axis, split_axis=split_dim, concat_axis=concat_dim, tiled=True
                )
            )
        )
    return jax.tree.map(lambda *parts: jnp.concatenate(parts, axis=out_dim), *done)


def expert_hidden(arrived, gate_weight, up_weight):
    gate_pre = jnp.einsum(
        "scd,df->scf", arrived, gate_weight[0], preferred_element_type=jnp.float32
    )
    up_pre = jnp.einsum("scd,df->scf", arrived, up_weight[0], preferred_element_type=jnp.float32)
    return (jax.nn.silu(gate_pre) * up_pre).astype(jnp.bfloat16)


def window_attention(query_rows, key_rows, value_rows, sink_logit):
    row_count = query_rows.shape[0]
    kv_here = key_rows.shape[1] // HEAD_DIM
    group_size = query_rows.shape[1] // (kv_here * HEAD_DIM)
    block_rows = min(512, row_count)
    joined = jnp.concatenate([key_rows, value_rows], axis=1)
    padded = padded_2(joined, (("ep", 0),), WINDOW)
    seq_total = row_count * lax.axis_size("ep")
    offset = lax.axis_index("ep") * row_count
    sink_col = sink_logit.reshape(kv_here, group_size)[:, :, None]
    score_scale = HEAD_DIM ** (-0.5)

    def one_block(block_index):
        first_row = block_index * block_rows
        query_block = lax.dynamic_slice_in_dim(query_rows, first_row, block_rows, 0).reshape(
            block_rows, kv_here, group_size, HEAD_DIM
        )
        key_span = lax.dynamic_slice_in_dim(padded, first_row, block_rows + 2 * WINDOW, 0)
        key_block = key_span[:, : kv_here * HEAD_DIM].reshape(-1, kv_here, HEAD_DIM)
        value_block = key_span[:, kv_here * HEAD_DIM :].reshape(-1, kv_here, HEAD_DIM)
        scores = (
            jnp.einsum("qkgd,skd->kgqs", query_block, key_block, preferred_element_type=jnp.float32)
            * score_scale
        )
        query_pos = first_row + jnp.arange(block_rows, dtype=jnp.int32)
        key_pos = first_row - WINDOW + jnp.arange(block_rows + 2 * WINDOW, dtype=jnp.int32)
        global_pos = offset + key_pos
        inside = (
            (jnp.abs(key_pos[None, :] - query_pos[:, None]) <= WINDOW)
            & (global_pos >= 0)[None, :]
            & (global_pos < seq_total)[None, :]
        )
        scores = jnp.where(inside, scores, -jnp.inf)
        row_peak = jnp.maximum(jnp.max(scores, axis=-1), sink_col)
        weights = jnp.exp(scores - row_peak[..., None])
        total_weight = jnp.sum(weights, axis=-1) + jnp.exp(sink_col - row_peak)
        attended = jnp.einsum(
            "kgqs,skd->qkgd",
            weights.astype(jnp.bfloat16),
            value_block,
            preferred_element_type=jnp.float32,
        )
        attended = attended / jnp.transpose(total_weight, (2, 0, 1))[..., None]
        return attended.reshape(block_rows, -1).astype(jnp.bfloat16)

    pieces = lax.map(one_block, jnp.arange(row_count // block_rows, dtype=jnp.int32))
    return pieces.reshape(row_count, -1)


def body(
    query_rows,
    key_rows,
    value_rows,
    sink_logit,
    out_weight,
    routed_rows,
    norm_gain,
    routing,
    route_weight,
    gate_weight,
    up_weight,
    down_weight,
):
    attended = window_attention(query_rows, key_rows, value_rows, sink_logit)
    projected = lax.psum_scatter(
        jnp.dot(attended, out_weight, preferred_element_type=jnp.float32).astype(jnp.bfloat16),
        "tp",
        scatter_dimension=0,
        tiled=True,
    )
    token_count, model_width = routed_rows.shape
    top_count = routing.shape[1]
    experts = lax.axis_size("ep")
    capacity = token_count * top_count * 9 // (8 * experts)
    values = routed_rows.astype(jnp.float32)
    normed = (
        values * lax.rsqrt(jnp.mean(values * values, axis=-1, keepdims=True) + EPS) * norm_gain
    ).astype(jnp.bfloat16)
    chosen = routing.reshape(-1)
    onehot = (chosen[:, None] == jnp.arange(experts, dtype=jnp.int32)[None, :]).astype(jnp.int32)
    before = jnp.cumsum(onehot, axis=0) - onehot
    slot_index = jnp.sum(before * onehot, axis=1)
    target = chosen * capacity + slot_index
    outgoing = (
        jnp.zeros((experts * capacity, model_width), jnp.bfloat16)
        .at[target]
        .set(jnp.repeat(normed, top_count, axis=0))
    )
    outgoing = outgoing.reshape(experts, capacity, model_width)

    def expert_sectioned(arrived):
        hidden = expert_hidden(
            lax.all_gather(arrived, "tp", axis=0, tiled=True), gate_weight, up_weight
        )
        rounded = jnp.einsum(
            "scf,fd->scd", hidden, down_weight[0], preferred_element_type=jnp.float32
        ).astype(jnp.bfloat16)
        summed = sum_at_owner(
            lax.optimization_barrier(rounded).astype(jnp.float32).astype(jnp.bfloat16), "tp", 0
        )
        return lax.all_to_all(
            summed.astype(jnp.bfloat16), "ep", split_axis=0, concat_axis=0, tiled=True
        ).astype(summed.dtype)

    results = items_in_groups(outgoing, "ep", 0, 0, expert_sectioned, 1, 1)
    slot_results = results.reshape(experts * capacity, model_width)
    picked = slot_results[target] * route_weight.reshape(-1)[:, None]
    expert_mix = jnp.sum(picked.reshape(token_count, top_count, model_width), axis=1).astype(
        jnp.bfloat16
    )
    return (projected, expert_mix)


def solution(mesh):
    in_specs = (
        P("ep", "tp"),
        P("ep", "tp"),
        P("ep", "tp"),
        P("tp"),
        P("tp", None),
        P(("ep", "tp"), None),
        P(),
        P(("ep", "tp"), None),
        P(("ep", "tp"), None),
        P("ep", None, "tp"),
        P("ep", None, "tp"),
        P("ep", "tp", None),
    )
    out_specs = (P(("ep", "tp"), None), P(("ep", "tp"), None))
    return jax.shard_map(body, mesh=mesh, in_specs=in_specs, out_specs=out_specs, check_vma=False)
```

profile of v0, /device:TPU:1, one launch (start us, length us, event | category | flops | bytes accessed | tf_op | source)
XLA Modules:
  0.0 271.3 jit_solution(11826062474658149984)
XLA Ops:
  13.8 3.2 %scatter_custom_fusion = bf16[288,2048]{1,0:T(8,128)(2,1)} fusion(s32[256]{0:T(256)S(1)} %bitcast.150, bf16[256,2048]{1,0:T(8,128)(2,1)S(1)} %reshape.297, bf16[]{:T(256)} %constant.86.clone.1), kind=kCustom, calls=%fused_computation.50 | custom fusion | bytes 1179650 | tf_op jit(solution)/shard_map/scatter | solution.py:153
  18.6 37.7 %all_to_all.15 = bf16[32,9,2048]{2,1,0:T(8,128)(2,1)S(1)} all-to-all(bf16[32,9,2048]{2,1,0:T(8,128)(2,1)S(1)} %reshape.279), channel_id=1, replica_groups=mesh['ep'=32,'tp'=4] {'ep'}, dimensions={0} | all-to-all | bytes 2359296 | tf_op jit(solution)/shard_map/all_to_all | solution.py:51
  58.2 2.5 collective-permute-start
  60.7 2.1 collective-permute-start.1
  62.8 3.1 %collective-permute-done.1 = bf16[128,128]{0,1:T(8,128)(2,1)S(1)} collective-permute-done((bf16[128,128]{0,1:T(8,128)(2,1)S(1)}, bf16[128,128]{0,1:T(8,128)(2,1)S(1)}, u32[]{:S(2)}, u32[]{:S(2)}) %collective-permute-start.1) | collective-permute-done | bytes 32800 | tf_op jit(solution)/shard_map/ppermute | solution.py:21
  66.0 26.8 %while.12 = (s32[]{:T(128)}, bf16[2,512,256]{2,1,0:T(8,128)(2,1)S(1)}, s32[2]{0:T(128)S(1)}, bf16[1280,128]{0,1:T(8,128)(2,1)S(1)}, s32[]{:T(128)}, /*index=5*/b...) while((s32[]{:T(128)}, ...), condition=%wide.region_3.4_spmd, body=%wide.region_0.3_spmd.sunk | while | flops 422191360 | bytes 48526672 | solution.py:112
  70.6 2.6 copy-done.2
  74.7 4.5 %fusion.71 = bf16[512,1,4,64]{0,3,2,1:T(8,128)(2,1)S(1)} fusion(f32[768,512,4]{1,0,2:T(8,128)} %copy-done.2, f32[4,512]{1,0:T(4,128)S(1)} %broadcast_maximum_fusion.2, pred[512,768]{0,1:T(8,128)(4,1)S(1)} %fusion.67, f32[512,4]{0,1:T(4,128)S(1)} %fusion.70, bf16[1280,128]{0,1:T(8,128)(2,1)S(1)} %get-tuple-element.222, s32[]{:T(128)S(6)} %select_n.57, ...), kind=kOutput, calls=%fused_computation.15.clone.1 | convolution fusion | flops 207880192 | bytes 7061512 | tf_op jit(solution)/shard_map/while/body/eval_jaxpr/kgqs,skd->qkgd/dot_general | solution.py:103
  84.0 2.6 copy-done.2
  88.0 4.6 %fusion.71 = bf16[512,1,4,64]{0,3,2,1:T(8,128)(2,1)S(1)} fusion(f32[768,512,4]{1,0,2:T(8,128)} %copy-done.2, f32[4,512]{1,0:T(4,128)S(1)} %broadcast_maximum_fusion.2, pred[512,768]{0,1:T(8,128)(4,1)S(1)} %fusion.67, f32[512,4]{0,1:T(4,128)S(1)} %fusion.70, bf16[1280,128]{0,1:T(8,128)(2,1)S(1)} %get-tuple-element.222, s32[]{:T(128)S(6)} %select_n.57, ...), kind=kOutput, calls=%fused_computation.15.clone.1 | convolution fusion | flops 207880192 | bytes 7061512 | tf_op jit(solution)/shard_map/while/body/eval_jaxpr/kgqs,skd->qkgd/dot_general | solution.py:103
  92.8 3.2 %convolution_convert_fusion = bf16[1024,2048]{1,0:T(8,128)(2,1)} fusion(bf16[1024,256]{1,0:T(8,128)(2,1)S(1)} %bitcast.146, bf16[256,2048]{1,0:T(8,128)(2,1)S(1)} %copy-done), kind=kOutput, calls=%fused_computation.43 | convolution fusion | flops 1075838976 | bytes 5767168 | tf_op jit(solution)/shard_map/dot_general | solution.py:132
  96.0 12.0 %all-gather.2.cloned.1.call-done = bf16[128,9,2048]{2,0,1:T(8,128)(2,1)} async-done(((bf16[32,9,2048]{2,0,1:T(8,128)(2,1)}), bf16[128,9,2048]{2,0,1:T(8,128)(2,1)}) %all-gather.2.cloned.1.call-update) | async-done | bytes 4718608 | tf_op jit(solution)/shard_map/all_gather | solution.py:159
  108.1 14.7 %fusion.28 = f32[128,9,1792]{2,0,1:T(8,128)} fusion(bf16[128,9,2048]{2,0,1:T(8,128)(2,1)} %all-gather.2.cloned.1.call-done, bf16[1,2048,1792]{2,1,0:T(8,128)(2,1)} %param.24), kind=kOutput, calls=%fused_computation.37 | convolution fusion | flops 8455716864 | bytes 20316160 | tf_op jit(solution)/shard_map/scd,df->scf/dot_general | solution.py:63
  122.7 28.4 %fusion.37 = bf16[128,9,2048]{2,0,1:T(8,128)(2,1)} fusion(bf16[1,1792,2048]{2,1,0:T(8,128)(2,1)} %param.25, f32[128,9,1792]{2,0,1:T(8,128)} %fusion.28, bf16[128,9,2048]{2,0,1:T(8,128)(2,1)} %all-gather.2.cloned.1.call-done, bf16[1,2048,1792]{2,1,0:T(8,128)(2,1)} %param.23), kind=kOutput, calls=%fused_computation.42 | convolution fusion | flops 16926179328 | bytes 32374784 | tf_op jit(solution)/shard_map/scf,fd->scd/dot_general | solution.py:161
  151.2 2.8 %copy.46 = bf16[4,32,9,2048]{3,1,2,0:T(8,128)(2,1)S(1)} copy(bf16[4,32,9,2048]{3,1,0,2:T(8,128)(2,1)} %bitcast.145) | data formatting | bytes 9437184 | tf_op jit(solution)/shard_map/reshape | solution.py:28
  154.0 56.9 %all_to_all.16 = bf16[4,32,9,2048]{3,1,2,0:T(8,128)(2,1)} all-to-all(bf16[4,32,9,2048]{3,1,2,0:T(8,128)(2,1)S(1)} %copy.46), channel_id=1, replica_groups=mesh['ep'=32,'tp'=4] {'tp'}, dimensions={0} | all-to-all | bytes 9437184 | tf_op jit(solution)/shard_map/all_to_all | solution.py:34
  210.9 3.3 %reduce_sum.55 = bf16[32,9,2048]{2,0,1:T(8,128)(2,1)S(1)} reduce(bf16[4,32,9,2048]{3,1,2,0:T(8,128)(2,1)} %all_to_all.16, bf16[]{:T(256)} %constant.86.clone.1), dimensions={0}, to_apply=%region_10.11 | reduce | flops 1769472 | bytes 5898242 | tf_op jit(solution)/shard_map/reduce_sum | solution.py:35
  214.2 2.0 copy.48
  216.3 9.0 %all-to-all-start.2 = ((bf16[32,9,2048]{2,1,0:T(8,128)(2,1)}), bf16[32,9,2048]{2,1,0:T(8,128)(2,1)}, u32[]{:S(2)}, u32[]{:S(2)}) async-start(bf16[32,9,2048]{2,1,0:T(8,128)(2,1)} %copy.48), calls=%async_computation.3 | async-start | bytes 4194304 | tf_op jit(solution)/shard_map/all_to_all | solution.py:167
  225.4 28.1 %all-to-all-done.2 = bf16[32,9,2048]{2,1,0:T(8,128)(2,1)} async-done(((bf16[32,9,2048]{2,1,0:T(8,128)(2,1)}), bf16[32,9,2048]{2,1,0:T(8,128)(2,1)}, u32[]{:S(2)}, u32[]{:S(2)}) %all-to-all-start.2) | async-done | bytes 1179680 | tf_op jit(solution)/shard_map/all_to_all | solution.py:167
  253.5 1.8 reshape.284
  255.3 2.7 gather_fusion
  258.0 2.5 gather.6
  260.5 3.9 %multiply_reduce_fusion = bf16[128,2048]{1,0:T(8,128)(2,1)} fusion(f32[128,2,2048]{2,1,0:T(2,128)S(1)} %gather.6, f32[128,2]{1,0:T(8,128)S(1)} %copy.49), kind=kLoop, calls=%fused_computation.44 | loop fusion | flops 786432 | bytes 2622464 | tf_op jit(solution)/shard_map/reduce_sum | solution.py:174
  (74 shorter events, 21.2 us)
Async XLA Ops:
  7.2 85.6 %copy-start = (bf16[256,2048]{1,0:T(8,128)(2,1)S(1)}, bf16[256,2048]{1,0:T(8,128)(2,1)}, u32[]{:S(2)}) copy-start(bf16[256,2048]{1,0:T(8,128)(2,1)} %param.18) | copy-start | bytes 3145732
  7.2 100.9 %all-gather.2.cloned.1.call-start = ((), (), s32[]{:S(2)}) async-start(), calls=%async_computation.5 | async-start | bytes 5898240 | tf_op jit(solution)/shard_map/all_gather | solution.py:159
  13.8 44.3 %copy-start.3 = (bf16[1024,64]{0,1:T(8,128)(2,1)S(1)}, bf16[1024,64]{0,1:T(8,128)(2,1)}, u32[]{:S(2)}) copy-start(bf16[1024,64]{0,1:T(8,128)(2,1)} %param.15) | copy-start | bytes 393220
  17.0 41.1 %copy-start.4 = (bf16[1024,64]{0,1:T(8,128)(2,1)S(1)}, bf16[1024,64]{0,1:T(8,128)(2,1)}, u32[]{:S(2)}) copy-start(bf16[1024,64]{0,1:T(8,128)(2,1)} %param.16) | copy-start | bytes 393220
  17.0 49.0 %copy-start.5 = (f32[4]{0:T(128)S(1)}, f32[4]{0:T(128)}, u32[]{:S(2)}) copy-start(f32[4]{0:T(128)} %param.17) | copy-start | bytes 52
  58.1 206.4 %reduce-scatter.2.cloned.1.call-start = ((), (), s32[]{:S(2)}) async-start(), calls=%async_computation.4 | async-start | bytes 5242880 | tf_op jit(solution)/shard_map/reduce_scatter | solution.py:131
  58.2 4.6 %collective-permute-start = (bf16[128,128]{0,1:T(8,128)(2,1)S(1)}, bf16[128,128]{0,1:T(8,128)(2,1)S(1)}, u32[]{:S(2)}, u32[]{:S(2)}) collective-permute-start(bf16[128,128]{0,1:T(8,128)(2,1)S(1)} %get-tuple-element.138), channel_id=1, source_target_pairs={{0,4},{4,8},{8,12},{12,16},{16,20},{20,24},{24,28},{28,32},{32,36}... | collective-permute-start | bytes 98312 | tf_op jit(solution)/shard_map/ppermute | solution.py:20
  60.7 5.2 %collective-permute-start.1 = (bf16[128,128]{0,1:T(8,128)(2,1)S(1)}, bf16[128,128]{0,1:T(8,128)(2,1)S(1)}, u32[]{:S(2)}, u32[]{:S(2)}) collective-permute-start(bf16[128,128]{0,1:T(8,128)(2,1)S(1)} %get-tuple-element.139), channel_id=1, source_target_pairs={{4,0},{8,4},{12,8},{16,12},{20,16},{24,20},{28,24},{32,28},{36,32}... | collective-permute-start | bytes 98312 | tf_op jit(solution)/shard_map/ppermute | solution.py:21
  70.5 2.7 copy-start.2
  83.9 2.7 copy-start.2
  210.9 14.4 %copy-start.6 = (f32[128,2]{0,1:T(2,128)S(1)}, f32[128,2]{0,1:T(2,128)}, u32[]{:S(2)}) copy-start(f32[128,2]{0,1:T(2,128)} %param.22) | copy-start | bytes 3076
  216.3 37.3 %all-to-all-start.2 = ((bf16[32,9,2048]{2,1,0:T(8,128)(2,1)}), bf16[32,9,2048]{2,1,0:T(8,128)(2,1)}, u32[]{:S(2)}, u32[]{:S(2)}) async-start(bf16[32,9,2048]{2,1,0:T(8,128)(2,1)} %copy.48), calls=%async_computation.3 | async-start | bytes 4194304 | tf_op jit(solution)/shard_map/all_to_all | solution.py:167
  255.3 9.2 %copy-start.1 = (bf16[256,2048]{1,0:T(8,128)(2,1)S(1)}, bf16[256,2048]{1,0:T(8,128)(2,1)}, u32[]{:S(2)}) copy-start(bf16[256,2048]{1,0:T(8,128)(2,1)} %param.18) | copy-start | bytes 3145732
Sparse Core Ops, SparseCore 0:
  58.2 49.8 all-gather.1
  111.0 47.3 reduce-scatter.1
where the time goes:
time: 273 us; the launch traced here: 271 us
  blocking collectives  94.6 us (35%)
  matrix products  57.9 us (21%)
  waiting for transfers between devices  43.3 us (16%)
  local copies, waits for them, and re-layouts  30.3 us (11%)
  other arithmetic  15.8 us (6%)
  between operations  14.3 us (5%)
  starting transfers between devices  13.7 us (5%)
    all_to_all x1, blocking collectives, sum_at_owner(): pieces = lax.all_to_all(split_up(value, dim, peers), axis, 0, 0, tiled=True)  56.9 us
    all_to_all x1, blocking collectives, items_in_groups(): lax.all_to_all(group, axis, split_axis=split_dim, concat_axis=concat_dim,...  37.7 us
    dot_general x1, matrix products, expert_sectioned(): jnp.einsum('scf,fd->scd', hidden, down_weight[0], preferred_element_type=...  28.4 us
    all_to_all x1, waiting for transfers between devices, expert_sectioned(): lax.all_to_all(summed.astype(jnp.bfloat16), 'ep', split_axis=0, concat_ax...  28.1 us
    dot_general x1, matrix products, expert_hidden(): jnp.einsum('scd,df->scf', arrived, up_weight[0], preferred_element_type=j...  14.7 us
    all_gather x1, waiting for transfers between devices, expert_sectioned(): lax.all_gather(arrived, 'tp', axis=0, tiled=True)  12 us
    dot_general x2, matrix products, one_block(): jnp.einsum('kgqs,skd->qkgd', weights.astype(jnp.bfloat16), value_block, p...  9.1 us
    all_to_all x1, starting transfers between devices, expert_sectioned(): lax.all_to_all(summed.astype(jnp.bfloat16), 'ep', split_axis=0, concat_ax...  9.03 us
  transfers between devices with their start and end apart: 5, of which 3 were waited for; matrix products, arithmetic and copies ran while one was open for 32% of the time, Pallas kernels for 0%

commit v1 on v0

v1 whole, which is shorter than its diff:
```python
import functools

import jax
import jax.numpy as jnp
from jax import lax
from jax.experimental import pallas as pl
from jax.experimental.pallas import tpu as pltpu
from jax.sharding import PartitionSpec as P

EPS = 1e-06
D = 2048
FF = 1792
EP = 32
TP = 4
NG = 4
GROUP = (0, 1, 3, 2)
BF = jnp.bfloat16
F32 = jnp.float32
MESH = pl.DeviceIdType.MESH


def rdma(src, dst, send_sem, recv_sem, device):
    return pltpu.make_async_remote_copy(
        src_ref=src,
        dst_ref=dst,
        send_sem=send_sem,
        recv_sem=recv_sem,
        device_id=device,
        device_id_type=MESH,
    )


def body(
    q_hbm, kv_hbm, sink, ow_hbm, rows_hbm, gain, route, rw, gw_hbm, uw_hbm, dw_hbm,
    mixed, mix,
    gw, uw, dw, rows, pack, packo, gat, rawo, gato, xc, hid, part,
    s2, r2, s1, s1e, arr, so, ro, arro, ret, reto, res, reso, wide,
    q, kv, ka, kb, va, vb, att, abuf, wo,
    ld, dsp_s, dsp_r, ag_s, ag_r, rs_s, rs_r, ret_s, ret_r, halo_s, halo_r, att_s, att_r, w_s, w_r,
):
    p = lax.axis_index("ep")
    x = lax.axis_index("tp")
    z, own = p // 8, p % 8
    core, chip = p % 2, p // 2
    right = (p, (x + 1) % TP)
    left = (p, (x + 3) % TP)
    across = (p, (x + 2) % TP)

    load_rows = pltpu.make_async_copy(rows_hbm, rows, ld.at[0])
    load_rows.start()
    load_kv = pltpu.make_async_copy(kv_hbm, kv.at[pl.ds(128, 1024)], ld.at[1])
    load_kv.start()
    load_q = pltpu.make_async_copy(q_hbm, q, ld.at[2])
    load_q.start()
    load_gw = pltpu.make_async_copy(gw_hbm.at[0], gw, ld.at[3])
    load_gw.start()
    load_uw = pltpu.make_async_copy(uw_hbm.at[0], uw, ld.at[4])
    load_uw.start()
    load_dw = pltpu.make_async_copy(dw_hbm.at[0], dw, ld.at[5])
    load_dw.start()
    load_ow = [
        pltpu.make_async_copy(ow_hbm.at[:, pl.ds(1024 * h, 1024)], wo.at[h, 0], ld.at[6 + h])
        for h in range(2)
    ]
    for c in load_ow:
        c.start()

    barrier = pltpu.get_barrier_semaphore()

    def greet(j, carry):
        pl.semaphore_signal(barrier, inc=1, device_id=((p + j) % EP, x), device_id_type=MESH)
        return carry

    lax.fori_loop(1, EP, greet, 0)
    for peer in (right, left, across):
        pl.semaphore_signal(barrier, inc=1, device_id=peer, device_id_type=MESH)

    lane32 = lax.broadcasted_iota(jnp.int32, (128, EP), 1)
    first, second = route[:, 0:1], route[:, 1:2]
    hot0 = (lane32 == first).astype(F32)
    hot1 = (lane32 == second).astype(F32)
    row_id = lax.broadcasted_iota(jnp.int32, (128, 128), 0)
    col_id = lax.broadcasted_iota(jnp.int32, (128, 128), 1)
    lower = (col_id < row_id).astype(BF)
    before = jnp.dot(lower, (hot0 + hot1).astype(BF), preferred_element_type=F32)
    slot0 = jnp.sum(before * hot0, axis=1, keepdims=True).astype(jnp.int32)
    slot1 = jnp.sum(before * hot1, axis=1, keepdims=True).astype(jnp.int32)
    place0 = jnp.where(slot0 < 8, first * 8 + slot0, 256 + first)
    place1 = jnp.where(slot1 < 8, second * 8 + slot1, 256 + second)
    lane = lax.broadcasted_iota(jnp.int32, (128, 384), 1)
    at0, at1 = lane == place0, lane == place1
    spread = jnp.where(at0 | at1, 1.0, 0.0).astype(F32)
    spread = jnp.transpose(spread).astype(BF)

    load_rows.wait()
    values = rows[...].astype(F32)
    scale = lax.rsqrt(jnp.mean(values * values, axis=-1, keepdims=True) + EPS)
    rows[...] = (values * scale * gain[...]).astype(BF)

    for c in range(8):
        cols = pl.ds(256 * c, 256)
        packed = jnp.dot(spread, rows[:, cols], preferred_element_type=F32)
        pack[:, :, cols] = packed[0:256].reshape(EP, 8, 256).astype(BF)
        wide[:, 2 * c, :] = packed[256:288, 0:128]
        wide[:, 2 * c + 1, :] = packed[256:288, 128:256]
    packo[...] = wide[...].astype(BF)
    gat[0, 0, own] = pack[p]
    rawo[0, own] = packo[p]

    pl.semaphore_wait(barrier, EP - 1 + TP - 1)

    after_me, before_me = (p + 1) % EP, (p + EP - 1) % EP
    halo_up = rdma(kv_hbm.at[pl.ds(896, 128)], kv.at[pl.ds(0, 128)], halo_s.at[0], halo_r.at[0], (after_me, x))
    halo_down = rdma(kv_hbm.at[pl.ds(0, 128)], kv.at[pl.ds(1152, 128)], halo_s.at[1], halo_r.at[1], (before_me, x))
    halo_up.start()
    halo_down.start()

    for k in range(NG):
        to = ((z + 4 - GROUP[k]) % 4) * 8

        def send(j, carry):
            e = to + (own + j) % 8
            rdma(pack.at[e], gat.at[k, 0, own], dsp_s.at[0], dsp_r.at[0, k], (e, x)).start()
            rdma(packo.at[e], rawo.at[k, own], dsp_s.at[1], dsp_r.at[1, k], (e, x)).start()
            return carry

        lax.fori_loop(1 if k == 0 else 0, 8, send, 0)

    half = pl.ds(pl.multiple_of(1024 * core, 1024), 1024)
    mine = pl.ds(pl.multiple_of(16 * chip, 16), 16)
    w_first = []
    for r in range(1, TP):
        c = rdma(ow_hbm.at[mine, half], wo.at[core, TP - r, mine], w_s.at[r - 1], w_r.at[r - 1], (p, (x + r) % TP))
        c.start()
        w_first.append(c)

    def arrive(k):
        low = 1 if k == 0 else 0
        n = 8 - low
        main, over = gat.at[k, 0, pl.ds(0, n)], rawo.at[k, pl.ds(0, n)]
        rdma(main, main, dsp_s.at[0], dsp_r.at[0, k], right).wait_recv()
        rdma(over, over, dsp_s.at[1], dsp_r.at[1, k], right).wait_recv()
        wide[0:8] = rawo[k].astype(F32)
        for c in range(16):
            gato[k, 0, :, 128 * c : 128 * c + 128] = wide[0:8, c, :].astype(BF)

    def ag_own(k):
        out = [
            rdma(gat.at[k, 0], gat.at[k, 3], ag_s.at[k, 0], ag_r.at[k, 0], right),
            rdma(gat.at[k, 0], gat.at[k, 1], ag_s.at[k, 1], ag_r.at[k, 1], left),
            rdma(gato.at[k, 0], gato.at[k, 3], ag_s.at[k, 2], ag_r.at[k, 2], right),
            rdma(gato.at[k, 0], gato.at[k, 1], ag_s.at[k, 3], ag_r.at[k, 3], left),
        ]
        for c in out:
            c.start()
        return out

    def ag_forward(k, sent):
        lo, hi = pl.ds(0, 4), pl.ds(4, 4)
        out = [
            rdma(gat.at[k, 3, lo], gat.at[k, 2, lo], ag_s.at[k, 4], ag_r.at[k, 4], right),
            rdma(gat.at[k, 1, hi], gat.at[k, 2, hi], ag_s.at[k, 5], ag_r.at[k, 5], left),
        ]
        if k % 2 == 0:
            out.append(rdma(gato.at[k, 3], gato.at[k, 2], ag_s.at[k, 6], ag_r.at[k, 6], right))
        else:
            out.append(rdma(gato.at[k, 1], gato.at[k, 2], ag_s.at[k, 6], ag_r.at[k, 6], left))
        sent[0].wait_recv()
        sent[2].wait_recv()
        out[0].start()
        if k % 2 == 0:
            out[2].start()
        sent[1].wait_recv()
        sent[3].wait_recv()
        out[1].start()
        if k % 2 == 1:
            out[2].start()
        return out

    qrow = lax.broadcasted_iota(jnp.int32, (256, 384), 0) % 128
    kcol = lax.broadcasted_iota(jnp.int32, (256, 384), 1)
    top_half = lax.broadcasted_iota(jnp.int32, (256, 1), 0) < 128
    lane128 = lax.broadcasted_iota(jnp.int32, (256, 128), 1)

    def attend(b, carry):
        at = pl.multiple_of(128 * b, 128)
        queries = q[pl.ds(at, 128), :]
        queries = jnp.concatenate([queries[:, 0:128], queries[:, 128:256]], axis=0)
        span = pl.ds(at, 384)
        is_first = ((p == 0) & (b == 0)).astype(jnp.int32)
        is_last = ((p == EP - 1) & (b == 7)).astype(jnp.int32)
        inside = (kcol >= jnp.maximum(qrow, 128 * is_first)) & (
            kcol <= jnp.minimum(qrow + 256, 383 - 128 * is_last)
        )
        outs, dens = [], []
        for keys, vals, h in ((ka, va, 0), (kb, vb, 1)):
            scores = lax.dot_general(
                queries, keys[span, :], (((1,), (1,)), ((), ())), preferred_element_type=F32
            )
            scores = jnp.where(inside, scores * 0.125, -jnp.inf)
            sink_col = jnp.where(top_half, sink[h], sink[2 + h])
            peak = jnp.maximum(jnp.max(scores, axis=1, keepdims=True), sink_col)
            weights = jnp.exp(scores - peak)
            dens.append(jnp.sum(weights, axis=1, keepdims=True) + jnp.exp(sink_col - peak))
            outs.append(jnp.dot(weights.astype(BF), vals[span, :], preferred_element_type=F32))
        total = (outs[0] + outs[1]) / jnp.where(lane128 < 64, dens[0], dens[1])
        total = total.astype(BF)
        att[pl.ds(at, 128), 0:128] = total[0:128]
        att[pl.ds(at, 128), 128:256] = total[128:256]
        return carry

    def split_kv(b, carry):
        at = pl.ds(pl.multiple_of(128 * b, 128), 128)
        both = kv[at, :].astype(F32)
        turned = pltpu.roll(both, 64, 1)
        low = lax.broadcasted_iota(jnp.int32, (128, 128), 1) < 64
        ka[at, :] = jnp.where(low, both, 0.0).astype(BF)
        kb[at, :] = jnp.where(low, 0.0, turned).astype(BF)
        va[at, :] = jnp.where(low, turned, 0.0).astype(BF)
        vb[at, :] = jnp.where(low, 0.0, both).astype(BF)
        return carry

    def expert(k):
        gathered, b = gat.at[k], k % 3

        def assemble(c, carry):
            cols = pl.ds(pl.multiple_of(256 * c, 256), 256)
            xc[0:256, cols] = gathered[:, :, :, cols].reshape(256, 256)
            xc[256:288, cols] = gato[k, :, :, cols].reshape(32, 256)
            return carry

        lax.fori_loop(0, 8, assemble, 0)

        def up(n, carry):
            cols = pl.ds(pl.multiple_of(256 * n, 256), 256)
            g = jnp.dot(xc[...], gw[:, cols], preferred_element_type=F32)
            u = jnp.dot(xc[...], uw[:, cols], preferred_element_type=F32)
            hid[:, cols] = (g / (1.0 + jnp.exp(-g)) * u).astype(BF)
            return carry

        lax.fori_loop(0, FF // 256, up, 0)

        def down(n, carry):
            cols = pl.ds(pl.multiple_of(256 * n, 256), 256)
            part[b, :, cols] = jnp.dot(hid[...], dw[:, cols], preferred_element_type=F32)
            return carry

        lax.fori_loop(0, D // 256, down, 0)

    def rs_first(k):
        b = k % 3
        s2[k, 0] = part[b, 128:160].astype(BF)
        s2[k, 1] = part[b, 160:192].astype(BF)
        s1[k, 0] = part[b, 96:128].astype(BF)
        s1[k, 1] = part[b, 192:224].astype(BF)
        so[k, 0] = part[b, 272:280].astype(BF)
        even = k % 2 == 0
        forward, back = (right, left) if even else (left, right)
        if even:
            so[k, 1] = part[b, 280:288].astype(BF)
        else:
            so[k, 1] = part[b, 264:272].astype(BF)
        out = [
            rdma(s2.at[k, 0], r2.at[k, 0], rs_s.at[k, 0], rs_r.at[k, 0], right),
            rdma(s2.at[k, 1], r2.at[k, 1], rs_s.at[k, 1], rs_r.at[k, 1], left),
            rdma(so.at[k, 0], ro.at[k], rs_s.at[k, 2], rs_r.at[k, 2], forward),
            rdma(s1.at[k, 0], arr.at[k, 0, pl.ds(32, 32)], rs_s.at[k, 3], rs_r.at[k, 3], right),
            rdma(s1.at[k, 1], arr.at[k, 1, pl.ds(0, 32)], rs_s.at[k, 4], rs_r.at[k, 4], left),
            rdma(so.at[k, 1], arro.at[k, 1], rs_s.at[k, 5], rs_r.at[k, 5], back),
        ]
        for c in out:
            c.start()
        return out

    def rs_second(k, sent):
        b = k % 3
        even = k % 2 == 0
        out = [
            rdma(s1e.at[k, 0], arr.at[k, 0, pl.ds(0, 32)], rs_s.at[k, 6], rs_r.at[k, 6], right),
            rdma(s1e.at[k, 1], arr.at[k, 1, pl.ds(32, 32)], rs_s.at[k, 7], rs_r.at[k, 7], left),
            rdma(so.at[k, 2], arro.at[k, 0], rs_s.at[k, 8], rs_r.at[k, 8], right if even else left),
        ]
        sent[0].wait_recv()
        s1e[k, 0] = (part[b, 64:96] + r2[k, 0].astype(F32)).astype(BF)
        out[0].start()
        sent[1].wait_recv()
        s1e[k, 1] = (part[b, 224:256] + r2[k, 1].astype(F32)).astype(BF)
        out[1].start()
        sent[2].wait_recv()
        at = 264 if even else 280
        so[k, 2] = (part[b, at : at + 8] + ro[k].astype(F32)).astype(BF)
        out[2].start()
        return out

    def finish(k, one, two):
        b = k % 3
        for c in (one[3], one[4], one[5], two[0], two[1], two[2]):
            c.wait_recv()
        total = part[b, 0:64] + arr[k, 0].astype(F32) + arr[k, 1].astype(F32)
        ret[k] = total.reshape(8, 8, D).astype(BF)
        ninth = part[b, 256:264] + arro[k, 0].astype(F32) + arro[k, 1].astype(F32)
        for c in range(16):
            wide[0:8, c, :] = ninth[:, 128 * c : 128 * c + 128]
        reto[k] = wide[0:8].astype(BF)
        to = ((z + GROUP[k]) % 4) * 8

        def send(j, carry):
            i = (own + j) % 8
            rdma(ret.at[k, i], res.at[p], ret_s.at[0], ret_r.at[0], (to + i, x)).start()
            rdma(reto.at[k, i], reso.at[p], ret_s.at[1], ret_r.at[1], (to + i, x)).start()
            return carry

        lax.fori_loop(1 if k == 0 else 0, 8, send, 0)
        if k == 0:
            res[p] = ret[0, own]
            reso[p] = reto[0, own]

    ag, fwd, one, two = {}, {}, {}, {}

    arrive(0)
    ag[0] = ag_own(0)

    load_kv.wait()
    halo_up.wait_recv()
    halo_down.wait_recv()
    lax.fori_loop(0, 10, split_kv, 0)
    load_q.wait()
    arrive(1)
    ag[1] = ag_own(1)

    for c in w_first:
        c.wait_recv()
    piece = wo.at[core, pl.ds(1, 3), mine]

    def w_send(i, carry):
        to = ((chip + i) % 16) * 2 + core
        rdma(piece, piece, w_s.at[3], w_r.at[3], (to, x)).start()
        return carry

    lax.fori_loop(1, 16, w_send, 0)

    lax.fori_loop(0, 4, attend, 0)
    fwd[0] = ag_forward(0, ag[0])
    arrive(2)
    ag[2] = ag_own(2)
    lax.fori_loop(4, 8, attend, 0)
    fwd[1] = ag_forward(1, ag[1])
    arrive(3)
    ag[3] = ag_own(3)

    att_sent = []
    for r in range(1, TP):
        to = (x + r) % TP
        c = rdma(
            att.at[pl.ds(pl.multiple_of(256 * to, 256), 256)],
            abuf.at[TP - r],
            att_s.at[r - 1],
            att_r.at[r - 1],
            (p, to),
        )
        c.start()
        att_sent.append(c)
    abuf[0] = att[pl.ds(pl.multiple_of(256 * x, 256), 256), :]

    load_gw.wait()
    load_uw.wait()
    load_dw.wait()
    for c in fwd[0]:
        c.wait_recv()
    expert(0)
    one[0] = rs_first(0)
    fwd[2] = ag_forward(2, ag[2])

    landed = wo.at[core, pl.ds(1, 3), pl.ds(0, 240)]
    rdma(landed, landed, w_s.at[3], w_r.at[3], right).wait_recv()
    w_half = wo.at[core, pl.ds(1, 3)]
    w_swap = rdma(w_half, w_half, w_s.at[4], w_r.at[4], (p + 1 - 2 * core, x))
    w_swap.start()

    for c in fwd[1]:
        c.wait_recv()
    expert(1)
    one[1] = rs_first(1)
    fwd[3] = ag_forward(3, ag[3])
    two[0] = rs_second(0, one[0])

    for c in att_sent:
        c.wait_recv()
    w_swap.wait_recv()
    for c in load_ow:
        c.wait()

    for h in range(2):

        def project(n, carry):
            cols = pl.ds(pl.multiple_of(256 * n, 256), 256)
            total = jnp.dot(abuf[0], wo[h, 0, :, cols], preferred_element_type=F32)
            for r in range(1, TP):
                total = total + jnp.dot(abuf[r], wo[h, r, :, cols], preferred_element_type=F32)
            mixed[:, pl.ds(pl.multiple_of(1024 * h + 256 * n, 256), 256)] = total.astype(BF)
            return carry

        lax.fori_loop(0, 4, project, 0)

    for c in fwd[2]:
        c.wait_recv()
    expert(2)
    one[2] = rs_first(2)
    two[1] = rs_second(1, one[1])
    finish(0, one[0], two[0])

    for c in fwd[3]:
        c.wait_recv()
    expert(3)
    one[3] = rs_first(3)
    two[2] = rs_second(2, one[2])
    finish(1, one[1], two[1])
    two[3] = rs_second(3, one[3])
    finish(2, one[2], two[2])
    finish(3, one[3], two[3])

    weight = jnp.where(at0, rw[:, 0:1], 0.0) + jnp.where(at1, rw[:, 1:2], 0.0)
    w_hi = weight.astype(BF)
    w_lo = (weight - w_hi.astype(F32)).astype(BF)
    back = res.at[pl.ds(0, EP - 1)]
    rdma(back, back, ret_s.at[0], ret_r.at[0], right).wait_recv()
    back = reso.at[pl.ds(0, EP - 1)]
    rdma(back, back, ret_s.at[1], ret_r.at[1], right).wait_recv()
    wide[...] = reso[...].astype(F32)
    for c in range(8):
        cols = pl.ds(256 * c, 256)
        slots = res[:, :, cols].reshape(256, 256)
        ninth = jnp.concatenate([wide[:, 2 * c, :], wide[:, 2 * c + 1, :]], axis=1).astype(BF)
        total = jnp.dot(w_hi[:, 0:256], slots, preferred_element_type=F32)
        total = total + jnp.dot(w_lo[:, 0:256], slots, preferred_element_type=F32)
        total = total + jnp.dot(w_hi[:, 256:288], ninth, preferred_element_type=F32)
        total = total + jnp.dot(w_lo[:, 256:288], ninth, preferred_element_type=F32)
        mix[:, cols] = total.astype(BF)

    halo_up.wait_send()
    halo_down.wait_send()
    for c in w_first + att_sent + [w_swap]:
        c.wait_send()
    for k in range(NG):
        for c in ag[k] + fwd[k] + one[k] + two[k]:
            c.wait_send()
    for ref, sem in ((pack, dsp_s.at[0]), (packo, dsp_s.at[1]), (res, ret_s.at[0]), (reso, ret_s.at[1])):
        sent = ref.at[pl.ds(0, EP - 1)]
        rdma(sent, sent, sem, sem, right).wait_send()
    rdma(landed, landed, w_s.at[3], w_r.at[3], right).wait_send()


def local(
    query_rows, key_rows, value_rows, sink_logit, out_weight, routed_rows, norm_gain, routing,
    route_weight, gate_weight, up_weight, down_weight,
):
    kv = jnp.concatenate([key_rows, value_rows], axis=1)
    anywhere = pl.BlockSpec(memory_space=pl.ANY)
    vmem = pl.BlockSpec(memory_space=pltpu.VMEM)
    smem = pl.BlockSpec(memory_space=pltpu.SMEM)
    dma = pltpu.SemaphoreType.DMA
    scratch = [
        pltpu.VMEM((D, FF), BF),
        pltpu.VMEM((D, FF), BF),
        pltpu.VMEM((FF, D), BF),
        pltpu.VMEM((128, D), BF),
        pltpu.VMEM((EP, 8, D), BF),
        pltpu.VMEM((EP, 16, 128), BF),
        pltpu.VMEM((NG, TP, 8, 8, D), BF),
        pltpu.VMEM((NG, 8, 16, 128), BF),
        pltpu.VMEM((NG, TP, 8, D), BF),
        pltpu.VMEM((288, D), BF),
        pltpu.VMEM((288, FF), BF),
        pltpu.VMEM((3, 288, D), F32),
        pltpu.VMEM((NG, 2, 32, D), BF),
        pltpu.VMEM((NG, 2, 32, D), BF),
        pltpu.VMEM((NG, 2, 32, D), BF),
        pltpu.VMEM((NG, 2, 32, D), BF),
        pltpu.VMEM((NG, 2, 64, D), BF),
        pltpu.VMEM((NG, 3, 8, D), BF),
        pltpu.VMEM((NG, 8, D), BF),
        pltpu.VMEM((NG, 2, 8, D), BF),
        pltpu.VMEM((NG, 8, 8, D), BF),
        pltpu.VMEM((NG, 8, 16, 128), BF),
        pltpu.VMEM((EP, 8, D), BF),
        pltpu.VMEM((EP, 16, 128), BF),
        pltpu.VMEM((EP, 16, 128), F32),
        pltpu.VMEM((1024, 256), BF),
        pltpu.VMEM((1280, 128), BF),
        pltpu.VMEM((1280, 128), BF),
        pltpu.VMEM((1280, 128), BF),
        pltpu.VMEM((1280, 128), BF),
        pltpu.VMEM((1280, 128), BF),
        pltpu.VMEM((1024, 256), BF),
        pltpu.VMEM((TP, 256, 256), BF),
        pltpu.VMEM((2, TP, 256, 1024), BF),
        dma((8,)),
        dma((2,)),
        dma((2, NG)),
        dma((NG, 7)),
        dma((NG, 7)),
        dma((NG, 9)),
        dma((NG, 9)),
        dma((2,)),
        dma((2,)),
        dma((2,)),
        dma((2,)),
        dma((3,)),
        dma((3,)),
        dma((5,)),
        dma((5,)),
    ]
    return pl.pallas_call(
        body,
        out_shape=(
            jax.ShapeDtypeStruct((256, D), BF),
            jax.ShapeDtypeStruct((128, D), BF),
        ),
        in_specs=[anywhere, anywhere, smem, anywhere, anywhere, vmem, vmem, vmem, anywhere, anywhere, anywhere],
        out_specs=(vmem, vmem),
        scratch_shapes=scratch,
        compiler_params=pltpu.CompilerParams(
            collective_id=0, has_side_effects=True, vmem_limit_bytes=66_000_000
        ),
        name="mixture",
    )(
        query_rows, kv, sink_logit, out_weight, routed_rows, norm_gain.reshape(1, D), routing,
        route_weight, gate_weight, up_weight, down_weight,
    )


def solution(mesh):
    in_specs = (
        P("ep", "tp"),
        P("ep", "tp"),
        P("ep", "tp"),
        P("tp"),
        P("tp", None),
        P(("ep", "tp"), None),
        P(),
        P(("ep", "tp"), None),
        P(("ep", "tp"), None),
        P("ep", None, "tp"),
        P("ep", None, "tp"),
        P("ep", "tp", None),
    )
    out_specs = (P(("ep", "tp"), None), P(("ep", "tp"), None))
    return jax.shard_map(local, mesh=mesh, in_specs=in_specs, out_specs=out_specs, check_vma=False)
```

time: 273 us -> 128 us (0.47)
  Pallas kernels: 0 us -> 116 us
  blocking collectives: 94.6 us -> 0 us
  matrix products: 57.9 us -> 0 us
  waiting for transfers between devices: 43.3 us -> 0 us
  local copies, waits for them, and re-layouts: 30.3 us -> 9.15 us
  other arithmetic: 15.8 us -> 0.85 us
  starting transfers between devices: 13.7 us -> 0 us
  between operations: 14.3 us -> 0.65 us
    pallas_call x0 -> x1, Pallas kernels: none -> 116 us  [local(): pl.pallas_call(body, out_shape=(jax.ShapeDtypeStruct((256, D), BF), jax.S...]
    all_to_all x2 -> x0, blocking collectives: 94.6 us -> none  [the longest x1 56.9 us: sum_at_owner(): pieces = lax.all_to_all(split_up(value, dim, peers), axis, 0, 0, tiled=True)]
    dot_general x7 -> x0, matrix products: 57.9 us -> none  [the longest x1 28.4 us: expert_sectioned(): jnp.einsum('scf,fd->scd', hidden, down_weight[0], preferred_element_type=...]
    all_to_all x1 -> x0, waiting for transfers between devices: 28.1 us -> none  [expert_sectioned(): lax.all_to_all(summed.astype(jnp.bfloat16), 'ep', split_axis=0, concat_ax...]
    all_gather x1 -> x0, waiting for transfers between devices: 12 us -> none  [expert_sectioned(): lax.all_gather(arrived, 'tp', axis=0, tiled=True)]
    reduce_sum x6 -> x0, other arithmetic: 11.3 us -> none  [the longest x1 3.93 us: body(): jnp.sum(picked.reshape(token_count, top_count, model_width), axis=1)]
    all_to_all x1 -> x0, starting transfers between devices: 9.03 us -> none  [expert_sectioned(): lax.all_to_all(summed.astype(jnp.bfloat16), 'ep', split_axis=0, concat_ax...]
    unnamed x15 -> x6, local copies, waits for them, and re-layouts: 1.02 us -> 9.15 us
  transfers between devices with their start and end apart: 5 -> 0, of which waited for: 3 -> 0; matrix products, arithmetic and copies ran while one was open for 32% -> 0% of each run, Pallas kernels for 0% -> 0%
where the time goes in v1:
time: 128 us; the launch traced here: 127 us
  Pallas kernels  116 us (91%)
  local copies, waits for them, and re-layouts  9.15 us (7%)
    pallas_call x1, Pallas kernels, local(): pl.pallas_call(body, out_shape=(jax.ShapeDtypeStruct((256, D), BF), jax.S...  116 us
    unnamed x6, local copies, waits for them, and re-layouts  9.15 us

profile of v1, /device:TPU:1, one launch (start us, length us, event | category | flops | bytes accessed | tf_op | source)
XLA Modules:
  0.0 126.6 jit_solution(842995888179177302)
XLA Ops:
  0.6 1.4 %copy.16.route = s32[128,2]{1,0:T(8,128)} copy(s32[128,2]{0,1:T(2,128)} %param.19) | data formatting | bytes 2048 | tf_op args[7]
  2.0 1.4 %copy.17.rw = f32[128,2]{1,0:T(8,128)} copy(f32[128,2]{0,1:T(2,128)} %param.20) | data formatting | bytes 2048 | tf_op args[8]
  3.5 1.1 copy.14
  4.5 1.1 copy.15
  5.6 0.9 pad_maximum_fusion.kv_hbm
  6.5 115.9 %mixture.1 = (bf16[256,2048]{1,0:T(8,128)(2,1)}, bf16[128,2048]{1,0:T(8,128)(2,1)}) custom-call(bf16[1024,256]{1,0:T(8,128)(2,1)} %q_hbm.1, bf16[1024,128]{1,0:T(8,128)(2,1)} %pad_maximum_fusion.kv_hbm, f32[4]{0:T(128)} %sink.1, bf16[256,2048]{1,0:T(8,128)(2,1)} %ow_hbm.1, bf16[128,2048]{1,0:T(8,128)(2,1)} %rows_hbm.1, f32[1,2048]{1,0:T(1,128)} %bitcast.1, ...), custom_call_target="tpu_custom_call" | custom-call | tf_op jit(solution)/shard_map/mixture/pallas_call | solution.py:513
  122.4 2.3 %copy.20 = bf16[256,2048]{1,0:T(8,128)(2,1)} copy(bf16[256,2048]{1,0:T(8,128)(2,1)} %get-tuple-element.4) | data formatting | bytes 2097152
  124.7 1.9 %copy.21 = bf16[128,2048]{1,0:T(8,128)(2,1)} copy(bf16[128,2048]{1,0:T(8,128)(2,1)} %get-tuple-element.5) | data formatting | bytes 1048576

commit v2 on v1

--- a/solution.py
+++ b/solution.py
@@ -13,7 +13,10 @@
 EP = 32
 TP = 4
 NG = 4
-GROUP = (0, 1, 3, 2)
+GROUP = (2, 1, 3, 0)
+HOME = GROUP.index(0)
+C2 = 768
+C1 = D - C2
 BF = jnp.bfloat16
 F32 = jnp.float32
 MESH = pl.DeviceIdType.MESH
@@ -31,12 +34,13 @@
 
 
 def body(
-    q_hbm, kv_hbm, sink, ow_hbm, rows_hbm, gain, route, rw, gw_hbm, uw_hbm, dw_hbm,
+    q_hbm, k_hbm, v_hbm, sink, ow_hbm, rows_hbm, gain, route, rw, gw_hbm, uw_hbm, dw_hbm,
     mixed, mix,
     gw, uw, dw, rows, pack, packo, gat, rawo, gato, xc, hid, part,
+    nt, peers, spread2, pack2, gat2,
     s2, r2, s1, s1e, arr, so, ro, arro, ret, reto, res, reso, wide,
     q, kv, ka, kb, va, vb, att, abuf, wo,
-    ld, dsp_s, dsp_r, ag_s, ag_r, rs_s, rs_r, ret_s, ret_r, halo_s, halo_r, att_s, att_r, w_s, w_r,
+    ld, dsp_s, dsp_r, ag_s, ag_r, rs_s, rs_r, ret_s, ret_r, halo_s, halo_r, att_s, att_r, w_s, w_r, nt_s, nt_r, pr_s, pr_r, d2_s, d2_r,
 ):
     p = lax.axis_index("ep")
     x = lax.axis_index("tp")
@@ -48,8 +52,12 @@
 
     load_rows = pltpu.make_async_copy(rows_hbm, rows, ld.at[0])
     load_rows.start()
-    load_kv = pltpu.make_async_copy(kv_hbm, kv.at[pl.ds(128, 1024)], ld.at[1])
-    load_kv.start()
+    load_kv = [
+        pltpu.make_async_copy(k_hbm, kv.at[pl.ds(0, 64), pl.ds(128, 1024)], ld.at[1]),
+        pltpu.make_async_copy(v_hbm, kv.at[pl.ds(64, 64), pl.ds(128, 1024)], ld.at[8]),
+    ]
+    for c in load_kv:
+        c.start()
     load_q = pltpu.make_async_copy(q_hbm, q, ld.at[2])
     load_q.start()
     load_gw = pltpu.make_async_copy(gw_hbm.at[0], gw, ld.at[3])
@@ -75,43 +83,64 @@
     for peer in (right, left, across):
         pl.semaphore_signal(barrier, inc=1, device_id=peer, device_id_type=MESH)
 
-    lane32 = lax.broadcasted_iota(jnp.int32, (128, EP), 1)
-    first, second = route[:, 0:1], route[:, 1:2]
-    hot0 = (lane32 == first).astype(F32)
-    hot1 = (lane32 == second).astype(F32)
-    row_id = lax.broadcasted_iota(jnp.int32, (128, 128), 0)
-    col_id = lax.broadcasted_iota(jnp.int32, (128, 128), 1)
-    lower = (col_id < row_id).astype(BF)
-    before = jnp.dot(lower, (hot0 + hot1).astype(BF), preferred_element_type=F32)
-    slot0 = jnp.sum(before * hot0, axis=1, keepdims=True).astype(jnp.int32)
-    slot1 = jnp.sum(before * hot1, axis=1, keepdims=True).astype(jnp.int32)
+    expert_id = lax.broadcasted_iota(jnp.int32, (EP, 128), 0)
+    earlier = lax.broadcasted_iota(jnp.int32, (128, 128), 0) < lax.broadcasted_iota(
+        jnp.int32, (128, 128), 1
+    )
+    earlier = jnp.where(earlier, 1.0, 0.0).astype(BF)
+
+    def slots(first, second):
+        hot0 = jnp.where(expert_id == first, 1.0, 0.0)
+        hot1 = jnp.where(expert_id == second, 1.0, 0.0)
+        before = jnp.dot((hot0 + hot1).astype(BF), earlier, preferred_element_type=F32)
+        slot0 = jnp.sum(before * hot0, axis=0, keepdims=True).astype(jnp.int32)
+        slot1 = jnp.sum(before * hot1, axis=0, keepdims=True).astype(jnp.int32)
+        return slot0, slot1
+
+    first, second = route[0:1, :], route[1:2, :]
+    slot0, slot1 = slots(first, second)
     place0 = jnp.where(slot0 < 8, first * 8 + slot0, 256 + first)
     place1 = jnp.where(slot1 < 8, second * 8 + slot1, 256 + second)
-    lane = lax.broadcasted_iota(jnp.int32, (128, 384), 1)
-    at0, at1 = lane == place0, lane == place1
-    spread = jnp.where(at0 | at1, 1.0, 0.0).astype(F32)
-    spread = jnp.transpose(spread).astype(BF)
+    slot_id = lax.broadcasted_iota(jnp.int32, (384, 128), 0)
+    at0, at1 = slot_id == place0, slot_id == place1
+    spread = jnp.where(at0 | at1, 1.0, 0.0).astype(BF)
 
     load_rows.wait()
     values = rows[...].astype(F32)
     scale = lax.rsqrt(jnp.mean(values * values, axis=-1, keepdims=True) + EPS)
     rows[...] = (values * scale * gain[...]).astype(BF)
 
-    for c in range(8):
+    pl.semaphore_wait(barrier, EP - 1 + TP - 1)
+
+    tail = rows.at[:, pl.ds(C1, C2)]
+    nt_sent = [
+        rdma(tail, nt.at[3], nt_s.at[0], nt_r.at[0], right),
+        rdma(tail, nt.at[1], nt_s.at[1], nt_r.at[1], left),
+    ]
+    pr_sent = [
+        rdma(route, peers.at[TP - r], pr_s.at[r - 1], pr_r.at[r - 1], (p, (x + r) % TP))
+        for r in range(1, TP)
+    ]
+    for c in pr_sent + nt_sent:
+        c.start()
+
+    for c in range(C1 // 256):
         cols = pl.ds(256 * c, 256)
-        packed = jnp.dot(spread, rows[:, cols], preferred_element_type=F32)
+        packed = jnp.dot(spread[0:288], rows[:, cols], preferred_element_type=F32)
         pack[:, :, cols] = packed[0:256].reshape(EP, 8, 256).astype(BF)
         wide[:, 2 * c, :] = packed[256:288, 0:128]
         wide[:, 2 * c + 1, :] = packed[256:288, 128:256]
+    for c in range(C1 // 128, 16):
+        wide[:, c, :] = jnp.zeros((EP, 128), F32)
     packo[...] = wide[...].astype(BF)
-    gat[0, 0, own] = pack[p]
-    rawo[0, own] = packo[p]
-
-    pl.semaphore_wait(barrier, EP - 1 + TP - 1)
-
+    gat[HOME, 0, own] = pack[p]
+    rawo[HOME, own] = packo[p]
+
+    for c in load_kv:
+        c.wait()
     after_me, before_me = (p + 1) % EP, (p + EP - 1) % EP
-    halo_up = rdma(kv_hbm.at[pl.ds(896, 128)], kv.at[pl.ds(0, 128)], halo_s.at[0], halo_r.at[0], (after_me, x))
-    halo_down = rdma(kv_hbm.at[pl.ds(0, 128)], kv.at[pl.ds(1152, 128)], halo_s.at[1], halo_r.at[1], (before_me, x))
+    halo_up = rdma(kv.at[:, pl.ds(1024, 128)], kv.at[:, pl.ds(0, 128)], halo_s.at[0], halo_r.at[0], (after_me, x))
+    halo_down = rdma(kv.at[:, pl.ds(128, 128)], kv.at[:, pl.ds(1152, 128)], halo_s.at[1], halo_r.at[1], (before_me, x))
     halo_up.start()
     halo_down.start()
 
@@ -124,7 +153,28 @@
             rdma(packo.at[e], rawo.at[k, own], dsp_s.at[1], dsp_r.at[1, k], (e, x)).start()
             return carry
 
-        lax.fori_loop(1 if k == 0 else 0, 8, send, 0)
+        lax.fori_loop(1 if k == HOME else 0, 8, send, 0)
+
+    for c in pr_sent:
+        c.wait_recv()
+    row_id = lax.broadcasted_iota(jnp.int32, (1280, 128), 0)
+    for r in range(TP):
+        a, b = (first, second) if r == 0 else (peers[r, 0:1, :], peers[r, 1:2, :])
+        sa, sb = slots(a, b)
+        pa = a * 40 + jnp.where(sa < 8, 8 * r + sa, 32 + r)
+        pb = b * 40 + jnp.where(sb < 8, 8 * r + sb, 32 + r)
+        spread2[:, 128 * r : 128 * r + 128] = jnp.where(
+            (row_id == pa) | (row_id == pb), 1.0, 0.0
+        ).astype(BF)
+    nt[0] = rows[:, C1:D]
+    upper, below = pl.ds(0, 64), pl.ds(64, 64)
+    nt_on = [
+        rdma(nt.at[3, upper], nt.at[2, upper], nt_s.at[2], nt_r.at[2], right),
+        rdma(nt.at[1, below], nt.at[2, below], nt_s.at[3], nt_r.at[3], left),
+    ]
+    for c, d in zip(nt_sent, nt_on):
+        c.wait_recv()
+        d.start()
 
     half = pl.ds(pl.multiple_of(1024 * core, 1024), 1024)
     mine = pl.ds(pl.multiple_of(16 * chip, 16), 16)
@@ -135,13 +185,13 @@
         w_first.append(c)
 
     def arrive(k):
-        low = 1 if k == 0 else 0
+        low = 1 if k == HOME else 0
         n = 8 - low
         main, over = gat.at[k, 0, pl.ds(0, n)], rawo.at[k, pl.ds(0, n)]
         rdma(main, main, dsp_s.at[0], dsp_r.at[0, k], right).wait_recv()
         rdma(over, over, dsp_s.at[1], dsp_r.at[1, k], right).wait_recv()
         wide[0:8] = rawo[k].astype(F32)
-        for c in range(16):
+        for c in range(C1 // 128):
             gato[k, 0, :, 128 * c : 128 * c + 128] = wide[0:8, c, :].astype(BF)
 
     def ag_own(k):
@@ -195,41 +245,50 @@
         outs, dens = [], []
         for keys, vals, h in ((ka, va, 0), (kb, vb, 1)):
             scores = lax.dot_general(
-                queries, keys[span, :], (((1,), (1,)), ((), ())), preferred_element_type=F32
+                queries, keys[:, span], (((1,), (0,)), ((), ())), preferred_element_type=F32
             )
             scores = jnp.where(inside, scores * 0.125, -jnp.inf)
             sink_col = jnp.where(top_half, sink[h], sink[2 + h])
             peak = jnp.maximum(jnp.max(scores, axis=1, keepdims=True), sink_col)
             weights = jnp.exp(scores - peak)
             dens.append(jnp.sum(weights, axis=1, keepdims=True) + jnp.exp(sink_col - peak))
-            outs.append(jnp.dot(weights.astype(BF), vals[span, :], preferred_element_type=F32))
+            outs.append(
+                lax.dot_general(
+                    weights.astype(BF),
+                    vals[:, span],
+                    (((1,), (1,)), ((), ())),
+                    preferred_element_type=F32,
+                )
+            )
         total = (outs[0] + outs[1]) / jnp.where(lane128 < 64, dens[0], dens[1])
         total = total.astype(BF)
         att[pl.ds(at, 128), 0:128] = total[0:128]
         att[pl.ds(at, 128), 128:256] = total[128:256]
         return carry
 
-    def split_kv(b, carry):
-        at = pl.ds(pl.multiple_of(128 * b, 128), 128)
-        both = kv[at, :].astype(F32)
-        turned = pltpu.roll(both, 64, 1)
-        low = lax.broadcasted_iota(jnp.int32, (128, 128), 1) < 64
-        ka[at, :] = jnp.where(low, both, 0.0).astype(BF)
-        kb[at, :] = jnp.where(low, 0.0, turned).astype(BF)
-        va[at, :] = jnp.where(low, turned, 0.0).astype(BF)
-        vb[at, :] = jnp.where(low, 0.0, both).astype(BF)
-        return carry
+    def split_kv():
+        none = jnp.zeros((64, 1280), BF)
+        ka[0:64], ka[64:128] = kv[0:64], none
+        kb[0:64], kb[64:128] = none, kv[0:64]
+        va[0:64], va[64:128] = kv[64:128], none
+        vb[0:64], vb[64:128] = none, kv[64:128]
 
     def expert(k):
         gathered, b = gat.at[k], k % 3
 
-        def assemble(c, carry):
-            cols = pl.ds(pl.multiple_of(256 * c, 256), 256)
+        for c in range(C1 // 256):
+            cols = pl.ds(256 * c, 256)
             xc[0:256, cols] = gathered[:, :, :, cols].reshape(256, 256)
             xc[256:288, cols] = gato[k, :, :, cols].reshape(32, 256)
-            return carry
-
-        lax.fori_loop(0, 8, assemble, 0)
+        to = lax.broadcasted_iota(jnp.int32, (32, 64), 0)
+        turn = lax.broadcasted_iota(jnp.int32, (32, 64), 1) == (to % 8) * 8 + to // 8
+        turn = jnp.where(turn, 1.0, 0.0).astype(BF)
+        for c in range(C2 // 256):
+            cols, at = pl.ds(256 * c, 256), pl.ds(C1 + 256 * c, 256)
+            for r in range(TP):
+                xc[64 * r : 64 * r + 64, at] = gat2[k, :, r, :, cols].reshape(64, 256)
+            ninth = gat2[k, :, 4, :, cols].reshape(64, 256)
+            xc[256:288, at] = jnp.dot(turn, ninth, preferred_element_type=F32).astype(BF)
 
         def up(n, carry):
             cols = pl.ds(pl.multiple_of(256 * n, 256), 256)
@@ -310,23 +369,46 @@
             rdma(reto.at[k, i], reso.at[p], ret_s.at[1], ret_r.at[1], (to + i, x)).start()
             return carry
 
-        lax.fori_loop(1 if k == 0 else 0, 8, send, 0)
-        if k == 0:
-            res[p] = ret[0, own]
-            reso[p] = reto[0, own]
+        lax.fori_loop(1 if k == HOME else 0, 8, send, 0)
+        if k == HOME:
+            res[p] = ret[k, own]
+            reso[p] = reto[k, own]
 
     ag, fwd, one, two = {}, {}, {}, {}
+
+    def pack_columns():
+        for i in range(4):
+            for c in range(C2 // 256):
+                cols = pl.ds(256 * c, 256)
+                packed = jnp.dot(
+                    spread2[320 * i : 320 * i + 320],
+                    nt[:, :, cols].reshape(512, 256),
+                    preferred_element_type=F32,
+                )
+                pack2[8 * i : 8 * i + 8, :, :, cols] = packed.reshape(8, 5, 8, 256).astype(BF)
+        gat2[HOME, own] = pack2[p]
+        for k in range(NG):
+            to = ((z + 4 - GROUP[k]) % 4) * 8
+
+            def send(j, carry):
+                e = to + (own + j) % 8
+                rdma(pack2.at[e], gat2.at[k, own], d2_s.at[0], d2_r.at[k], (e, x)).start()
+                return carry
+
+            lax.fori_loop(1 if k == HOME else 0, 8, send, 0)
+
+    def arrive2(k):
+        low = 1 if k == HOME else 0
+        slabs = gat2.at[k, pl.ds(0, 8 - low)]
+        rdma(slabs, slabs, d2_s.at[0], d2_r.at[k], right).wait_recv()
 
     arrive(0)
     ag[0] = ag_own(0)
-
-    load_kv.wait()
-    halo_up.wait_recv()
-    halo_down.wait_recv()
-    lax.fori_loop(0, 10, split_kv, 0)
-    load_q.wait()
     arrive(1)
     ag[1] = ag_own(1)
+    for c in nt_on:
+        c.wait_recv()
+    pack_columns()
 
     for c in w_first:
         c.wait_recv()
@@ -339,14 +421,21 @@
 
     lax.fori_loop(1, 16, w_send, 0)
 
-    lax.fori_loop(0, 4, attend, 0)
-    fwd[0] = ag_forward(0, ag[0])
     arrive(2)
     ag[2] = ag_own(2)
-    lax.fori_loop(4, 8, attend, 0)
-    fwd[1] = ag_forward(1, ag[1])
+    fwd[0] = ag_forward(0, ag[0])
     arrive(3)
     ag[3] = ag_own(3)
+    fwd[1] = ag_forward(1, ag[1])
+
+    halo_up.wait_recv()
+    halo_down.wait_recv()
+    split_kv()
+    load_q.wait()
+    lax.fori_loop(0, 4, attend, 0)
+    fwd[2] = ag_forward(2, ag[2])
+    lax.fori_loop(4, 8, attend, 0)
+    fwd[3] = ag_forward(3, ag[3])
 
     att_sent = []
     for r in range(1, TP):
@@ -367,9 +456,9 @@
     load_dw.wait()
     for c in fwd[0]:
         c.wait_recv()
+    arrive2(0)
     expert(0)
     one[0] = rs_first(0)
-    fwd[2] = ag_forward(2, ag[2])
 
     landed = wo.at[core, pl.ds(1, 3), pl.ds(0, 240)]
     rdma(landed, landed, w_s.at[3], w_r.at[3], right).wait_recv()
@@ -379,9 +468,9 @@
 
     for c in fwd[1]:
         c.wait_recv()
+    arrive2(1)
     expert(1)
     one[1] = rs_first(1)
-    fwd[3] = ag_forward(3, ag[3])
     two[0] = rs_second(0, one[0])
 
     for c in att_sent:
@@ -404,6 +493,7 @@
 
     for c in fwd[2]:
         c.wait_recv()
+    arrive2(2)
     expert(2)
     one[2] = rs_first(2)
     two[1] = rs_second(1, one[1])
@@ -411,6 +501,7 @@
 
     for c in fwd[3]:
         c.wait_recv()
+    arrive2(3)
     expert(3)
     one[3] = rs_first(3)
     two[2] = rs_second(2, one[2])
@@ -419,7 +510,8 @@
     finish(2, one[2], two[2])
     finish(3, one[3], two[3])
 
-    weight = jnp.where(at0, rw[:, 0:1], 0.0) + jnp.where(at1, rw[:, 1:2], 0.0)
+    weight = jnp.where(at0, rw[0:1, :], 0.0) + jnp.where(at1, rw[1:2, :], 0.0)
+    weight = jnp.transpose(weight)
     w_hi = weight.astype(BF)
     w_lo = (weight - w_hi.astype(F32)).astype(BF)
     back = res.at[pl.ds(0, EP - 1)]
@@ -439,22 +531,36 @@
 
     halo_up.wait_send()
     halo_down.wait_send()
-    for c in w_first + att_sent + [w_swap]:
+    for c in w_first + att_sent + [w_swap] + nt_sent + nt_on + pr_sent:
         c.wait_send()
     for k in range(NG):
         for c in ag[k] + fwd[k] + one[k] + two[k]:
             c.wait_send()
-    for ref, sem in ((pack, dsp_s.at[0]), (packo, dsp_s.at[1]), (res, ret_s.at[0]), (reso, ret_s.at[1])):
+    for ref, sem in ((pack, dsp_s.at[0]), (packo, dsp_s.at[1]), (res, ret_s.at[0]), (reso, ret_s.at[1]), (pack2, d2_s.at[0])):
         sent = ref.at[pl.ds(0, EP - 1)]
         rdma(sent, sent, sem, sem, right).wait_send()
     rdma(landed, landed, w_s.at[3], w_r.at[3], right).wait_send()
+
+
+def deliver(mixed_in, mix_in, mixed_out, mix_out, buf, sem_in, sem_out):
+    ins, outs = [], []
+    for i in range(6):
+        src, dst, at = (mixed_in, mixed_out, 64 * i) if i < 4 else (mix_in, mix_out, 64 * i - 256)
+        here = buf.at[pl.ds(64 * i, 64)]
+        ins.append(pltpu.make_async_copy(src.at[pl.ds(at, 64)], here, sem_in.at[i]))
+        outs.append(pltpu.make_async_copy(here, dst.at[pl.ds(at, 64)], sem_out.at[i]))
+        ins[i].start()
+    for i in range(6):
+        ins[i].wait()
+        outs[i].start()
+    for c in outs:
+        c.wait()
 
 
 def local(
     query_rows, key_rows, value_rows, sink_logit, out_weight, routed_rows, norm_gain, routing,
     route_weight, gate_weight, up_weight, down_weight,
 ):
-    kv = jnp.concatenate([key_rows, value_rows], axis=1)
     anywhere = pl.BlockSpec(memory_space=pl.ANY)
     vmem = pl.BlockSpec(memory_space=pltpu.VMEM)
     smem = pl.BlockSpec(memory_space=pltpu.SMEM)
@@ -464,14 +570,19 @@
         pltpu.VMEM((D, FF), BF),
         pltpu.VMEM((FF, D), BF),
         pltpu.VMEM((128, D), BF),
-        pltpu.VMEM((EP, 8, D), BF),
+        pltpu.VMEM((EP, 8, C1), BF),
         pltpu.VMEM((EP, 16, 128), BF),
-        pltpu.VMEM((NG, TP, 8, 8, D), BF),
+        pltpu.VMEM((NG, TP, 8, 8, C1), BF),
         pltpu.VMEM((NG, 8, 16, 128), BF),
-        pltpu.VMEM((NG, TP, 8, D), BF),
+        pltpu.VMEM((NG, TP, 8, C1), BF),
         pltpu.VMEM((288, D), BF),
         pltpu.VMEM((288, FF), BF),
         pltpu.VMEM((3, 288, D), F32),
+        pltpu.VMEM((TP, 128, C2), BF),
+        pltpu.VMEM((TP, 2, 128), jnp.int32),
+        pltpu.VMEM((1280, 512), BF),
+        pltpu.VMEM((EP, 5, 8, C2), BF),
+        pltpu.VMEM((NG, 8, 5, 8, C2), BF),
         pltpu.VMEM((NG, 2, 32, D), BF),
         pltpu.VMEM((NG, 2, 32, D), BF),
         pltpu.VMEM((NG, 2, 32, D), BF),
@@ -486,15 +597,15 @@
         pltpu.VMEM((EP, 16, 128), BF),
         pltpu.VMEM((EP, 16, 128), F32),
         pltpu.VMEM((1024, 256), BF),
-        pltpu.VMEM((1280, 128), BF),
-        pltpu.VMEM((1280, 128), BF),
-        pltpu.VMEM((1280, 128), BF),
-        pltpu.VMEM((1280, 128), BF),
-        pltpu.VMEM((1280, 128), BF),
+        pltpu.VMEM((128, 1280), BF),
+        pltpu.VMEM((128, 1280), BF),
+        pltpu.VMEM((128, 1280), BF),
+        pltpu.VMEM((128, 1280), BF),
+        pltpu.VMEM((128, 1280), BF),
         pltpu.VMEM((1024, 256), BF),
         pltpu.VMEM((TP, 256, 256), BF),
         pltpu.VMEM((2, TP, 256, 1024), BF),
-        dma((8,)),
+        dma((9,)),
         dma((2,)),
         dma((2, NG)),
         dma((NG, 7)),
@@ -509,14 +620,20 @@
         dma((3,)),
         dma((5,)),
         dma((5,)),
+        dma((4,)),
+        dma((4,)),
+        dma((3,)),
+        dma((3,)),
+        dma((1,)),
+        dma((NG,)),
     ]
-    return pl.pallas_call(
+    made = pl.pallas_call(
         body,
         out_shape=(
             jax.ShapeDtypeStruct((256, D), BF),
             jax.ShapeDtypeStruct((128, D), BF),
         ),
-        in_specs=[anywhere, anywhere, smem, anywhere, anywhere, vmem, vmem, vmem, anywhere, anywhere, anywhere],
+        in_specs=[anywhere, anywhere, anywhere, smem, anywhere, anywhere, vmem, vmem, vmem, anywhere, anywhere, anywhere],
         out_specs=(vmem, vmem),
         scratch_shapes=scratch,
         compiler_params=pltpu.CompilerParams(
@@ -524,9 +641,20 @@
         ),
         name="mixture",
     )(
-        query_rows, kv, sink_logit, out_weight, routed_rows, norm_gain.reshape(1, D), routing,
-        route_weight, gate_weight, up_weight, down_weight,
+        query_rows, key_rows.T, value_rows.T, sink_logit, out_weight, routed_rows,
+        norm_gain.reshape(1, D), routing.T, route_weight.T, gate_weight, up_weight, down_weight,
     )
+    return pl.pallas_call(
+        deliver,
+        out_shape=(
+            jax.ShapeDtypeStruct((256, D), BF),
+            jax.ShapeDtypeStruct((128, D), BF),
+        ),
+        in_specs=[anywhere, anywhere],
+        out_specs=(anywhere, anywhere),
+        scratch_shapes=[pltpu.VMEM((384, D), BF), dma((6,)), dma((6,))],
+        name="deliver",
+    )(*made)
 
 
 def solution(mesh):

time: 128 us -> 134 us (1.047)
  the two profiles are of different devices: /device:TPU:1 before, /device:TPU:33 now
where the time goes in v2:
time: 134 us
  Pallas kernels  133 us (99%)
    pallas_call x1, Pallas kernels, local(): pl.pallas_call(body, out_shape=(jax.ShapeDtypeStruct((256, D), BF), jax.S...  131 us

profile of v2, /device:TPU:33, one launch (start us, length us, event | category | flops | bytes accessed | tf_op | source)
XLA Modules:
  0.0 134.0 jit_solution(3664731934916367908)
XLA Ops:
  0.6 131.2 %mixture.1 = (bf16[256,2048]{1,0:T(8,128)(2,1)}, bf16[128,2048]{1,0:T(8,128)(2,1)}) custom-call(bf16[1024,256]{1,0:T(8,128)(2,1)} %q_hbm.1, bf16[64,1024]{1,0:T(8,128)(2,1)} %bitcast.5, bf16[64,1024]{1,0:T(8,128)(2,1)} %bitcast.6, f32[4]{0:T(128)} %sink.1, bf16[256,2048]{1,0:T(8,128)(2,1)} %ow_hbm.1, bf16[128,2048]{1,0:T(8,128)(2,1)} %rows_hbm.1, ...), custom_call_target="tpu_custom_call" | custom-call | tf_op jit(solution)/shard_map/mixture/pallas_call | solution.py:630
  131.8 2.2 %deliver.1 = (bf16[256,2048]{1,0:T(8,128)(2,1)}, bf16[128,2048]{1,0:T(8,128)(2,1)}) custom-call(bf16[256,2048]{1,0:T(8,128)(2,1)} %get-tuple-element.4.mixed_in, bf16[128,2048]{1,0:T(8,128)(2,1)} %get-tuple-element.5.mix_in), custom_call_target="tpu_custom_call" | custom-call | tf_op jit(solution)/shard_map/deliver/pallas_call | solution.py:647
